TPU v7x, 32 devices: a whole 2x2x4 slice. The times are simulated.
32 devices in a mesh: kv: 4 (over y, x), tp: 8 (over z, core).
Axes of the slice: x: 2, y: 2, z: 4, core: 2. Of those that a mesh axis runs over, the one named last changes fastest.
Arguments:
- tokens: bfloat16 [256, 4096], P('tp', 'kv'), may hold values from -19 to 19, as said below
- lengths: int32 [256], P('kv'), may hold values from 1 to 16384, 1048576 in all
- state_block: float32 [256, 64, 2048], P('kv', None, 'tp'), may hold values from -6 to 6
- cached_keys: bfloat16 [256, 128, 2048], P('kv', None, 'tp'), may hold values from -0.75 to 0.75
- cached_values: bfloat16 [256, 128, 2048], P('kv', None, 'tp'), may hold values from -6 to 6
- query_weight: bfloat16 [4096, 2048], P('kv', 'tp'), may hold values from -0.09375 to 0.09375
- key_weight: bfloat16 [4096, 2048], P('kv', 'tp'), may hold values from -0.09375 to 0.09375
- value_weight: bfloat16 [4096, 2048], P('kv', 'tp'), may hold values from -0.09375 to 0.09375
- gate_weight: bfloat16 [4096, 2048], P('kv', 'tp'), may hold values from -0.09375 to 0.09375
- decay_rate: float32 [32], P('tp'), may hold values from 0.0005 to 0.05
- head_gain: float32 [2048], P('tp'), may hold values from 0.1 to 1.9
- out_weight: bfloat16 [2048, 4096], P('tp', 'kv'), may hold values from -0.125 to 0.125
- mixer_gain: float32 [4096], P('kv'), may hold values from 0.1 to 1.9
- up_weight: bfloat16 [4096, 16384], P('kv', 'tp'), may hold values from -0.09375 to 0.09375
- down_weight: bfloat16 [16384, 4096], P('tp', 'kv'), may hold values from -0.046875 to 0.046875
- final_gain: float32 [4096], P('kv'), may hold values from 0.1 to 1.9
Outputs:
- next_rows: bfloat16 [256, 4096], P('tp', 'kv')
Inputs may be any that keep to these rules, and one draw needn't show every extreme that they name: `tokens`: the rows' column groups have scales that differ between groups.
All inputs are finite; a program needn't handle non-finite values. No bound on the sum of `lengths` on one device may be relied on, other than what follows from the above.
Results may differ from a plain program's by a relative error of at most 0.0095.
Values may be sent and summed in bfloat16 or wider, within the bound.
A program may use at most 128 MiB of HBM per device.

v0:
```python
import jax
import jax.numpy as jnp
from jax import lax
from jax.sharding import PartitionSpec as P

HDIM = 64
BLK = 128


ALPHA = 2.0**0.5
EPS = 1e-05


def rotate(vectors, positions):
    half = vectors.shape[-1] // 2
    inverse = 10000.0 ** (-jnp.arange(half, dtype=jnp.float32) / half)
    angle = positions.astype(jnp.float32)[:, None] * inverse[None, :]
    cosine = jnp.cos(angle)[:, None, :]
    sine = jnp.sin(angle)[:, None, :]
    former, latter = (vectors[..., :half], vectors[..., half:])
    return jnp.concatenate([former * cosine - latter * sine, latter * cosine + former * sine], -1)


def normalize(values, gain):
    width = values.shape[1] * lax.axis_size("kv")
    total, square = lax.psum((jnp.sum(values, 1), jnp.sum(values * values, 1)), "kv")
    mean = total / width
    centred = values - mean[:, None]
    spread = square / width - mean * mean
    return centred * lax.rsqrt(spread[:, None] + EPS) * gain[None, :]


def retain(query, keyed, valued, gated, lengths, state, keys, values, rate, gain):
    count = query.shape[0]
    heads = rate.shape[0]
    q_rot = rotate(query.astype(jnp.float32).reshape(count, heads, HDIM), lengths).astype(
        jnp.bfloat16
    )
    k_rot = (rotate(keyed.astype(jnp.float32).reshape(count, heads, HDIM), lengths) * 0.125).astype(
        jnp.bfloat16
    )
    v_new = valued.astype(jnp.float32).reshape(count, heads, HDIM)
    cached_k = keys.reshape(count, BLK, heads, HDIM)
    cached_v = values.reshape(count, BLK, heads, HDIM)
    scores = jnp.einsum("shn,sihn->shi", q_rot, cached_k, preferred_element_type=jnp.float32)
    offset = lengths % BLK
    slots = jnp.arange(BLK, dtype=jnp.int32)
    lag = jnp.maximum(offset[:, None] - slots[None, :], 0).astype(jnp.float32)
    live = (slots[None, :] < offset[:, None])[:, None, :]
    factor = jnp.where(live, jnp.exp(-rate[None, :, None] * lag[:, None, :]), 0.0)
    weights = (scores * factor).astype(jnp.bfloat16)
    own = jnp.einsum("shn,shn->sh", q_rot, k_rot, preferred_element_type=jnp.float32).astype(
        jnp.bfloat16
    )
    inner = jnp.einsum("shi,sihn->shn", weights, cached_v, preferred_element_type=jnp.float32)
    inner = inner + own.astype(jnp.float32)[..., None] * v_new
    carried = jnp.exp(-rate[None, :] * (offset[:, None] + 1).astype(jnp.float32))
    cross = (
        jnp.einsum(
            "shk,skhv->shv",
            q_rot.astype(jnp.float32),
            state.reshape(count, HDIM, heads, HDIM),
            precision=lax.Precision.HIGHEST,
        )
        * carried[..., None]
    )
    retained = inner + cross
    mean = jnp.mean(retained, -1, keepdims=True)
    centred = retained - mean
    spread = jnp.mean(centred * centred, -1, keepdims=True)
    normed = centred * lax.rsqrt(spread + EPS) * gain.reshape(heads, HDIM)[None]
    gate_f = jax.nn.silu(gated.astype(jnp.float32).reshape(count, heads, HDIM))
    return (gate_f * normed).reshape(count, heads * HDIM).astype(jnp.bfloat16)


def per_device(
    tokens,
    lengths,
    state_block,
    cached_keys,
    cached_values,
    query_weight,
    key_weight,
    value_weight,
    gate_weight,
    decay_rate,
    head_gain,
    out_weight,
    mixer_gain,
    up_weight,
    down_weight,
    final_gain,
):
    all_rows = lax.all_gather(tokens, "tp", axis=0, tiled=True)
    width = query_weight.shape[1]
    piece = all_rows
    summed = lax.psum_scatter(
        jnp.concatenate(
            [
                jnp.dot(piece, weight, preferred_element_type=jnp.float32)
                for weight in (query_weight, key_weight, value_weight, gate_weight)
            ],
            1,
        ),
        "kv",
        scatter_dimension=0,
        tiled=True,
    ).astype(jnp.bfloat16)
    query, keyed, valued, gated = [
        summed[:, index * width : (index + 1) * width] for index in range(4)
    ]
    mixed = retain(
        query,
        keyed,
        valued,
        gated,
        lengths,
        state_block,
        cached_keys,
        cached_values,
        decay_rate,
        head_gain,
    )
    mixed_all = lax.all_gather(mixed, "kv", axis=0, tiled=True)
    piece = mixed_all
    branch = lax.psum_scatter(
        jnp.dot(piece, out_weight, preferred_element_type=jnp.float32),
        "tp",
        scatter_dimension=0,
        tiled=True,
    )
    hidden = normalize(ALPHA * tokens.astype(jnp.float32) + branch, mixer_gain).astype(jnp.bfloat16)
    hidden_all = lax.all_gather(hidden, "tp", axis=0, tiled=True)
    upward = lax.psum(jnp.dot(hidden_all, up_weight, preferred_element_type=jnp.float32), "kv")
    active = jnp.square(jax.nn.relu(upward)).astype(jnp.bfloat16)
    piece = active
    downward = lax.psum_scatter(
        jnp.dot(piece, down_weight, preferred_element_type=jnp.float32),
        "tp",
        scatter_dimension=0,
        tiled=True,
    )
    result = normalize(ALPHA * hidden.astype(jnp.float32) + downward, final_gain)
    return result.astype(jnp.bfloat16)


def solution(mesh):
    return jax.shard_map(
        per_device,
        mesh=mesh,
        in_specs=(
            P("tp", "kv"),
            P("kv"),
            P("kv", None, "tp"),
            P("kv", None, "tp"),
            P("kv", None, "tp"),
            P("kv", "tp"),
            P("kv", "tp"),
            P("kv", "tp"),
            P("kv", "tp"),
            P("tp"),
            P("tp"),
            P("tp", "kv"),
            P("kv"),
            P("kv", "tp"),
            P("tp", "kv"),
            P("kv"),
        ),
        out_specs=P("tp", "kv"),
        check_vma=False,
    )
```

profile of v0, /device:TPU:0, one launch (start us, length us, event | category | flops | bytes accessed | tf_op | source)
XLA Modules:
  0.0 271.9 jit_solution(15027838848131162646)
XLA Ops:
  6.5 16.8 %all_gather.9 = bf16[256,1024]{1,0:T(8,128)(2,1)S(1)} all-gather(bf16[32,1024]{1,0:T(8,128)(2,1)} %param.16), channel_id=1, replica_groups=mesh['kv'=4,'tp'=8] {'tp'}, dimensions={0}, use_global_device_ids=true | all-gather | bytes 589824 | tf_op jit(solution)/shard_map/all_gather | solution.py:94
  23.4 1.4 fusion.22
  24.8 1.4 fusion.23
  26.2 1.4 fusion.24
  28.0 1.3 copy.37
  29.4 6.4 %copy.19 = bf16[64,128,256]{1,2,0:T(8,128)(2,1)} copy(bf16[64,128,256]{2,1,0:T(8,128)(2,1)} %param.19) | data formatting | bytes 8388608 | tf_op args[3]
  35.8 6.4 %copy.20 = bf16[64,128,256]{1,2,0:T(8,128)(2,1)} copy(bf16[64,128,256]{2,1,0:T(8,128)(2,1)} %param.20) | data formatting | bytes 8388608 | tf_op args[4]
  42.2 8.2 %reshape.187 = f32[64,64,4,64]{3,2,1,0:T(4,128)} reshape(f32[64,64,256]{2,1,0:T(8,128)} %param.18) | data formatting | bytes 8388608 | tf_op jit(solution)/shard_map/reshape | solution.py:62
  50.8 7.7 %reduce-scatter.10.cloned.1.call-done = f32[64,1024]{1,0:T(8,128)} async-done(((f32[256,1024]{1,0:T(8,128)}), f32[64,1024]{1,0:T(8,128)}) %reduce-scatter.10.cloned.1.call-update) | async-done | bytes 262160
  60.0 3.5 %fusion.26 = f32[64,4,1,128]{3,2,1,0:T(1,128)S(1)} fusion(bf16[64,4,64,1]{2,3,1,0:T(2,128)(2,1)S(1)} %copy.22, bf16[64,128,4,64]{1,3,2,0:T(8,128)(2,1)} %bitcast.41), kind=kOutput, calls=%fused_computation.63 | convolution fusion | flops 4194304 | bytes 4358144 | tf_op jit(solution)/shard_map/shn,sihn->shi/dot_general | solution.py:45
  63.7 2.3 fusion.9
  66.1 1.9 copy.39
  68.0 6.4 %multiply_reduce_fusion = f32[64,4,64]{2,1,0:T(4,128)S(1)} fusion(f32[64,64,4,64]{3,2,1,0:T(4,128)} %reshape.187, f32[64,4,64]{1,2,0:T(8,128)S(1)} %copy.39), kind=kLoop, calls=%fused_computation | loop fusion | flops 2080768 | bytes 4325376
  74.8 8.5 %all_gather.10 = bf16[256,256]{1,0:T(8,128)(2,1)S(1)} all-gather(bf16[64,256]{1,0:T(8,128)(2,1)S(1)} %copy.36), channel_id=1, replica_groups=mesh['kv'=4,'tp'=8] {'kv'}, dimensions={0}, use_global_device_ids=true | all-gather | bytes 163840 | tf_op jit(solution)/shard_map/all_gather | solution.py:124
  83.3 1.3 fusion.27
  84.7 32.7 %reduce-scatter.6.cloned.1.call-done = f32[32,1024]{1,0:T(8,128)} async-done(((f32[256,1024]{1,0:T(8,128)}), f32[32,1024]{1,0:T(8,128)}) %reduce-scatter.6.cloned.1.call-update) | async-done | bytes 131088 | tf_op jit(solution)/shard_map/reduce_scatter | solution.py:126
  118.4 9.9 %all-reduce.1 = (f32[32]{0:T(128)S(1)}, f32[32]{0:T(128)S(1)}) all-reduce(f32[32]{0:T(128)S(1)} %get-tuple-element.8, f32[32]{0:T(128)S(1)} %get-tuple-element.7), channel_id=1, replica_groups=mesh['kv'=4,'tp'=8] {'kv'}, use_global_device_ids=true, to_apply=%region_7.8 | all-reduce | flops 64 | bytes 512 | tf_op jit(solution)/shard_map/psum | solution.py:26
  129.3 14.9 %all_gather.11 = bf16[256,1024]{1,0:T(8,128)(2,1)S(1)} all-gather(bf16[32,1024]{1,0:T(8,128)(2,1)S(1)} %multiply_convert_fusion.3), channel_id=1, replica_groups=mesh['kv'=4,'tp'=8] {'tp'}, dimensions={0}, use_global_device_ids=true | all-gather | bytes 589824 | tf_op jit(solution)/shard_map/all_gather | solution.py:133
  144.2 4.8 %fusion.28 = f32[256,2048]{1,0:T(8,128)} fusion(bf16[256,1024]{1,0:T(8,128)(2,1)S(1)} %all_gather.11, bf16[1024,2048]{1,0:T(8,128)(2,1)} %param.29), kind=kOutput, calls=%fused_computation.65 | convolution fusion | flops 1073741824 | bytes 6815744 | tf_op jit(solution)/shard_map/dot_general | solution.py:134
  149.0 66.0 %all-reduce.4.cloned.1.call-done = f32[256,2048]{1,0:T(8,128)} async-done(((f32[256,2048]{1,0:T(8,128)}), f32[256,2048]{1,0:T(8,128)}) %all-reduce.4.cloned.1.call-update) | async-done | bytes 2097168 | tf_op jit(solution)/shard_map/psum | solution.py:134
  215.1 5.1 %fusion = f32[256,1024]{1,0:T(8,128)} fusion(bf16[2048,1024]{1,0:T(8,128)(2,1)} %param.30, f32[256,2048]{1,0:T(8,128)} %all-reduce.4.cloned.1.call-done), kind=kOutput, calls=%fused_computation.2 | convolution fusion | flops 1075314688 | bytes 7340032 | tf_op jit(solution)/shard_map/dot_general | solution.py:138
  220.1 32.7 %reduce-scatter.8.cloned.1.call-done = f32[32,1024]{1,0:T(8,128)} async-done(((f32[256,1024]{1,0:T(8,128)}), f32[32,1024]{1,0:T(8,128)}) %reduce-scatter.8.cloned.1.call-update) | async-done | bytes 131088 | tf_op jit(solution)/shard_map/reduce_scatter | solution.py:137
  253.9 9.8 %all-reduce = (f32[32]{0:T(128)S(1)}, f32[32]{0:T(128)S(1)}) all-reduce(f32[32]{0:T(128)S(1)} %get-tuple-element.6, f32[32]{0:T(128)S(1)} %get-tuple-element.5), channel_id=1, replica_groups=mesh['kv'=4,'tp'=8] {'kv'}, use_global_device_ids=true, to_apply=%region_13.14 | all-reduce | flops 64 | bytes 512 | tf_op jit(solution)/shard_map/psum | solution.py:26
  263.8 1.6 multiply_convert_fusion.2
  (59 shorter events, 6.3 us)
Async XLA Ops:
  6.5 76.7 %copy-start = (bf16[256,1024]{1,0:T(8,128)(2,1)S(1)}, bf16[256,1024]{1,0:T(8,128)(2,1)}, u32[]{:S(2)}) copy-start(bf16[256,1024]{1,0:T(8,128)(2,1)} %param.27) | copy-start | bytes 1572868
  6.5 21.0 %copy-start.3 = (bf16[1024,256]{1,0:T(8,128)(2,1)S(1)}, bf16[1024,256]{1,0:T(8,128)(2,1)}, u32[]{:S(2)}) copy-start(bf16[1024,256]{1,0:T(8,128)(2,1)} %param.24) | copy-start | bytes 1572868
  6.5 52.0 %reduce-scatter.10.cloned.1.call-start = ((), (), s32[]{:S(2)}) async-start(), calls=%async_computation.6 | async-start | bytes 1310720
  29.3 6.5 %copy-start.8 = (f32[4]{0:T(128)S(1)}, f32[4]{0:T(128)}, u32[]{:S(2)}) copy-start(f32[4]{0:T(128)} %param.25) | copy-start | bytes 52
  29.4 88.0 %reduce-scatter.6.cloned.1.call-start = ((), (), s32[]{:S(2)}) async-start(), calls=%async_computation.3 | async-start | bytes 1179648 | tf_op jit(solution)/shard_map/reduce_scatter | solution.py:126
  42.2 8.2 %copy-start.6 = (f32[256]{0:T(256)S(1)}, f32[256]{0:T(256)}, u32[]{:S(2)}) copy-start(f32[256]{0:T(256)} %param.26) | copy-start | bytes 3076
  42.2 8.3 %copy-start.7 = (s32[64]{0:T(128)S(1)}, s32[64]{0:T(128)}, u32[]{:S(2)}) copy-start(s32[64]{0:T(128)} %param.17) | copy-start | bytes 772
  60.0 3.7 %copy-start.1 = (bf16[64,128,256]{1,2,0:T(8,128)(2,1)S(1)}, bf16[64,128,256]{1,2,0:T(8,128)(2,1)}, u32[]{:S(2)}) copy-start(bf16[64,128,256]{1,2,0:T(8,128)(2,1)} %copy.20) | copy-start | bytes 12582916
  74.3 43.0 %copy-start.2 = (bf16[32,1024]{1,0:T(8,128)(2,1)S(1)}, bf16[32,1024]{1,0:T(8,128)(2,1)}, u32[]{:S(2)}) copy-start(bf16[32,1024]{1,0:T(8,128)(2,1)} %param.16) | copy-start | bytes 196612
  74.4 53.9 %copy-start.4 = (f32[1024]{0:T(1024)S(1)}, f32[1024]{0:T(1024)}, u32[]{:S(2)}) copy-start(f32[1024]{0:T(1024)} %param.28) | copy-start | bytes 12292
  84.6 130.5 %all-reduce.4.cloned.1.call-start = ((), (), s32[]{:S(2)}) async-start(), calls=%async_computation.4 | async-start | bytes 4194304 | tf_op jit(solution)/shard_map/psum | solution.py:134
  149.0 114.8 %copy-start.5 = (f32[1024]{0:T(1024)S(1)}, f32[1024]{0:T(1024)}, u32[]{:S(2)}) copy-start(f32[1024]{0:T(1024)} %param.31) | copy-start | bytes 12292
  149.0 103.9 %reduce-scatter.8.cloned.1.call-start = ((), (), s32[]{:S(2)}) async-start(), calls=%async_computation.5 | async-start | bytes 1179648 | tf_op jit(solution)/shard_map/reduce_scatter | solution.py:137
Sparse Core Ops, SparseCore 0:
  29.5 29.0 reduce-scatter.9
  84.7 32.5 reduce-scatter.5
  149.1 65.9 all-reduce.3
  220.3 32.5 reduce-scatter.7
where the time goes:
time: 273 us; the launch traced here: 272 us
  waiting for transfers between devices  139 us (51%)
  blocking collectives  60 us (22%)
  local copies, waits for them, and re-layouts  25.8 us (9%)
  matrix products  21.4 us (8%)
  between operations  13.4 us (5%)
  other arithmetic  12 us (4%)
    psum x1, waiting for transfers between devices, per_device(): lax.psum(jnp.dot(hidden_all, up_weight, preferred_element_type=jnp.float3...  66 us
    reduce_scatter x1, waiting for transfers between devices, per_device(): lax.psum_scatter(jnp.dot(piece, down_weight, preferred_element_type=jnp.f...  32.7 us
    reduce_scatter x1, waiting for transfers between devices, per_device(): lax.psum_scatter(jnp.dot(piece, out_weight, preferred_element_type=jnp.fl...  32.7 us
    psum x2, blocking collectives, normalize(): lax.psum((jnp.sum(values, 1), jnp.sum(values * values, 1)), 'kv')  19.7 us
    unnamed x23, local copies, waits for them, and re-layouts  17.2 us
    all_gather x1, blocking collectives, per_device(): all_rows = lax.all_gather(tokens, 'tp', axis=0, tiled=True)  16.8 us
    all_gather x1, blocking collectives, per_device(): hidden_all = lax.all_gather(hidden, 'tp', axis=0, tiled=True)  14.9 us
    all_gather x1, blocking collectives, per_device(): mixed_all = lax.all_gather(mixed, 'kv', axis=0, tiled=True)  8.47 us
  transfers between devices with their start and end apart: 4, of which 4 were waited for; matrix products, arithmetic and copies ran while one was open for 8% of the time, Pallas kernels for 0%

commit v1 on v0

v1 whole, which is shorter than its diff:
```python
import jax
import jax.numpy as jnp
from jax import lax
from jax.experimental import pallas as pl
from jax.experimental.pallas import tpu as pltpu
from jax.sharding import PartitionSpec as P

HDIM = 64
BLK = 128
TILE = 256

ALPHA = 2.0**0.5
EPS = 1e-05
MESH = pl.DeviceIdType.MESH
F32 = jnp.float32
BF16 = jnp.bfloat16


def peer_of(axis, step):
    size = lax.axis_size(axis)
    return lax.rem(lax.axis_index(axis) + step, size)


def enter(axes):
    barrier = pltpu.get_barrier_semaphore()
    total = 0
    for axis in axes:
        for step in range(1, lax.axis_size(axis)):
            pl.semaphore_signal(
                barrier, inc=1, device_id={axis: peer_of(axis, step)}, device_id_type=MESH
            )
            total += 1
    pl.semaphore_wait(barrier, total)


def remote(axis, step, src, dst, sems, index):
    return pltpu.make_async_remote_copy(
        src_ref=src,
        dst_ref=dst,
        send_sem=sems.at[(0, *index, step - 1)],
        recv_sem=sems.at[(1, *index, step - 1)],
        device_id={axis: peer_of(axis, step)},
        device_id_type=MESH,
    )


class Gather:
    def __init__(self, axis, src, held, sems, index=()):
        me = lax.axis_index(axis)
        self.copies = [
            remote(axis, step, src, held.at[me], sems, index)
            for step in range(1, lax.axis_size(axis))
        ]

    def start(self):
        for copy in self.copies:
            copy.start()

    def wait_recv(self):
        for copy in self.copies:
            copy.wait_recv()

    def wait_send(self):
        for copy in self.copies:
            copy.wait_send()


class Scatter(Gather):
    def __init__(self, axis, parts, landed, sems, index=()):
        self.copies = [
            remote(axis, step, parts.at[peer_of(axis, step)], landed.at[step - 1], sems, index)
            for step in range(1, lax.axis_size(axis))
        ]
        self.own = parts.at[lax.axis_index(axis)]
        self.landed = landed

    def total(self):
        return self.own[...].astype(F32) + jnp.sum(self.landed[...].astype(F32), 0)


def project_kernel(tokens, *refs):
    weights, (out, rows, held, parts, landed, tok_sems, part_sems, load_sems) = refs[:4], refs[4:]
    loads = [
        pltpu.make_async_copy(weight, held.at[index], load_sems.at[index])
        for index, weight in enumerate(weights)
    ]
    for load in loads:
        load.start()
    enter(("tp", "kv"))
    gather = Gather("tp", tokens, rows, tok_sems)
    gather.start()
    rows[lax.axis_index("tp")] = tokens[...]
    gather.wait_recv()
    count, block, depth = rows.shape
    width = held.shape[2]
    seqs = parts.shape[2]
    sends = []
    for index in range(4):
        loads[index].wait()
        part = jnp.dot(
            rows[...].reshape(count * block, depth), held[index], preferred_element_type=F32
        )
        parts[index] = part.astype(BF16).reshape(-1, seqs, width)
        send = Scatter("kv", parts.at[index], landed.at[index], part_sems, (index,))
        send.start()
        sends.append(send)
    for index, send in enumerate(sends):
        send.wait_recv()
        out[:, index * width : (index + 1) * width] = send.total().astype(BF16)
    gather.wait_send()
    for send in sends:
        send.wait_send()


def project(tokens, *weights):
    ntp, nkv = lax.axis_size("tp"), lax.axis_size("kv")
    block, depth = tokens.shape
    width = weights[0].shape[1]
    seqs = block * ntp // nkv
    return pl.pallas_call(
        project_kernel,
        name="project",
        out_shape=jax.ShapeDtypeStruct((seqs, 4 * width), BF16),
        in_specs=[pl.BlockSpec(memory_space=pltpu.VMEM)] + [pl.BlockSpec(memory_space=pl.ANY)] * 4,
        out_specs=pl.BlockSpec(memory_space=pltpu.VMEM),
        scratch_shapes=[
            pltpu.VMEM((ntp, block, depth), BF16),
            pltpu.VMEM((4, depth, width), BF16),
            pltpu.VMEM((4, nkv, seqs, width), BF16),
            pltpu.VMEM((4, nkv - 1, seqs, width), BF16),
            pltpu.SemaphoreType.DMA((2, ntp - 1)),
            pltpu.SemaphoreType.DMA((2, 4, nkv - 1)),
            pltpu.SemaphoreType.DMA((4,)),
        ],
        compiler_params=pltpu.CompilerParams(
            collective_id=0, has_side_effects=True, vmem_limit_bytes=60 * 2**20
        ),
    )(tokens, *weights)


def normalize(values, gain, mine, landed, sems):
    width = values.shape[1]
    nkv = lax.axis_size("kv")
    mean = jnp.mean(values, 1, keepdims=True)
    off = values - mean
    square = jnp.sum(off * off, 1, keepdims=True)
    lane = lax.broadcasted_iota(jnp.int32, mine.shape, 1)
    mine[...] = jnp.where(lane < 64, mean, square)
    copies = [
        remote("kv", step, mine, landed.at[step - 1], sems, ()) for step in range(1, nkv)
    ]
    for copy in copies:
        copy.start()
    for copy in copies:
        copy.wait_recv()
    others = [(landed[i, :, 0:1], landed[i, :, 64:65]) for i in range(nkv - 1)]
    means = [mean] + [pair[0] for pair in others]
    overall = sum(means) / nkv
    spread = square + sum(pair[1] for pair in others)
    spread = spread + width * sum((m - overall) * (m - overall) for m in means)
    spread = spread / (width * nkv)
    for copy in copies:
        copy.wait_send()
    return (values - overall) * lax.rsqrt(spread + EPS) * gain[...]


def mixer_kernel(
    mixed, tokens, out_w, mixer_gain, up_w, down_w, final_gain, out,
    out_v, up_v, down_v, heads, branch_parts, branch_landed, stat_mine, stat_landed,
    hidden_mine, hidden_all, up_parts, up_landed, act_mine, act_all, down_sum,
    load_sems, mix_sems, branch_sems, stat_sems, hid_sems, up_sems, act_sems, down_sems,
):
    loads = [
        pltpu.make_async_copy(src, dst, load_sems.at[index])
        for index, (src, dst) in enumerate(((out_w, out_v), (up_w, up_v), (down_w, down_v)))
    ]
    for load in loads:
        load.start()
    enter(("tp", "kv"))
    nkv, seqs, width = heads.shape
    tp, kv = lax.axis_index("tp"), lax.axis_index("kv")
    ntp, block, depth = hidden_all.shape
    gather = Gather("kv", mixed, heads, mix_sems)
    gather.start()
    heads[kv] = mixed[...]
    loads[0].wait()
    gather.wait_recv()
    part = jnp.dot(heads[...].reshape(nkv * seqs, width), out_v[...], preferred_element_type=F32)
    branch_parts[0] = part.astype(BF16).reshape(ntp, block, depth)
    branch = Scatter("tp", branch_parts.at[0], branch_landed.at[0], branch_sems)
    branch.start()
    branch.wait_recv()
    values = ALPHA * tokens[...].astype(F32) + branch.total()
    hidden = normalize(values, mixer_gain, stat_mine.at[0], stat_landed.at[0], stat_sems.at[0])
    hidden_mine[...] = hidden.astype(BF16)
    spread = Gather("tp", hidden_mine, hidden_all, hid_sems)
    spread.start()
    hidden_all[tp] = hidden_mine[...]
    loads[1].wait()
    spread.wait_recv()
    tiles, tile = up_parts.shape[0], up_parts.shape[3]

    def up_scatter(index):
        return Scatter("kv", up_parts.at[index], up_landed.at[index], up_sems.at[index])

    def act_gather(index):
        return Gather("kv", act_mine.at[index], act_all.at[index], act_sems.at[index])

    @pl.loop(0, tiles)
    def _(index):
        columns = pl.ds(pl.multiple_of(index * tile, tile), tile)
        part = jnp.dot(
            hidden_all[...].reshape(ntp * block, depth), up_v[:, columns],
            preferred_element_type=F32,
        )
        up_parts[index] = part.astype(BF16).reshape(nkv, seqs, tile)
        up_scatter(index).start()

    @pl.loop(0, tiles)
    def _(index):
        send = up_scatter(index)
        send.wait_recv()
        act_mine[index] = jnp.square(jnp.maximum(send.total(), 0.0)).astype(BF16)
        act_gather(index).start()
        act_all[index, kv] = act_mine[index]

    loads[2].wait()
    down_sum[...] = jnp.zeros_like(down_sum)

    @pl.loop(0, tiles)
    def _(index):
        act_gather(index).wait_recv()
        down_sum[...] += jnp.dot(
            act_all[index].reshape(nkv * seqs, tile),
            down_v[pl.ds(pl.multiple_of(index * tile, tile), tile), :],
            preferred_element_type=F32,
        )

    branch_parts[1] = down_sum[...].astype(BF16).reshape(ntp, block, depth)
    downward = Scatter("tp", branch_parts.at[1], branch_landed.at[1], down_sems)
    downward.start()
    downward.wait_recv()
    values = ALPHA * hidden_mine[...].astype(F32) + downward.total()
    result = normalize(values, final_gain, stat_mine.at[1], stat_landed.at[1], stat_sems.at[1])
    out[...] = result.astype(BF16)
    for group in (gather, branch, spread, downward):
        group.wait_send()

    @pl.loop(0, tiles)
    def _(index):
        up_scatter(index).wait_send()
        act_gather(index).wait_send()


def mixer(mixed, tokens, out_w, mixer_gain, up_w, down_w, final_gain):
    ntp, nkv = lax.axis_size("tp"), lax.axis_size("kv")
    seqs, width = mixed.shape
    block, depth = tokens.shape
    inner = up_w.shape[1]
    tile = min(TILE, inner)
    tiles = inner // tile
    vmem, anyw = pl.BlockSpec(memory_space=pltpu.VMEM), pl.BlockSpec(memory_space=pl.ANY)
    dma = pltpu.SemaphoreType.DMA
    return pl.pallas_call(
        mixer_kernel,
        name="mixer",
        out_shape=jax.ShapeDtypeStruct((block, depth), BF16),
        in_specs=[vmem, vmem, anyw, vmem, anyw, anyw, vmem],
        out_specs=vmem,
        scratch_shapes=[
            pltpu.VMEM((width, depth), BF16),
            pltpu.VMEM((depth, inner), BF16),
            pltpu.VMEM((inner, depth), BF16),
            pltpu.VMEM((nkv, seqs, width), BF16),
            pltpu.VMEM((2, ntp, block, depth), BF16),
            pltpu.VMEM((2, ntp - 1, block, depth), BF16),
            pltpu.VMEM((2, block, 128), F32),
            pltpu.VMEM((2, nkv - 1, block, 128), F32),
            pltpu.VMEM((block, depth), BF16),
            pltpu.VMEM((ntp, block, depth), BF16),
            pltpu.VMEM((tiles, nkv, seqs, tile), BF16),
            pltpu.VMEM((tiles, nkv - 1, seqs, tile), BF16),
            pltpu.VMEM((tiles, seqs, tile), BF16),
            pltpu.VMEM((tiles, nkv, seqs, tile), BF16),
            pltpu.VMEM((ntp * block, depth), F32),
            dma((3,)),
            dma((2, nkv - 1)),
            dma((2, ntp - 1)),
            dma((2, 2, nkv - 1)),
            dma((2, ntp - 1)),
            dma((tiles, 2, nkv - 1)),
            dma((tiles, 2, nkv - 1)),
            dma((2, ntp - 1)),
        ],
        compiler_params=pltpu.CompilerParams(
            collective_id=1, has_side_effects=True, vmem_limit_bytes=60 * 2**20
        ),
    )(mixed, tokens, out_w, mixer_gain[None, :], up_w, down_w, final_gain[None, :])


def rotate(vectors, positions):
    half = vectors.shape[-1] // 2
    inverse = 10000.0 ** (-jnp.arange(half, dtype=F32) / half)
    angle = positions.astype(F32)[:, None] * inverse[None, :]
    cosine = jnp.cos(angle)[:, None, :]
    sine = jnp.sin(angle)[:, None, :]
    former, latter = (vectors[..., :half], vectors[..., half:])
    return jnp.concatenate([former * cosine - latter * sine, latter * cosine + former * sine], -1)


def retain(query, keyed, valued, gated, lengths, state, keys, values, rate, gain):
    count, width = query.shape
    heads = rate.shape[0]
    q_rot = rotate(query.astype(F32).reshape(count, heads, HDIM), lengths).astype(BF16)
    k_rot = (rotate(keyed.astype(F32).reshape(count, heads, HDIM), lengths) * 0.125).astype(BF16)
    v_new = valued.astype(F32).reshape(count, heads, HDIM)
    owner = jnp.arange(width, dtype=jnp.int32)[None, :] // HDIM == jnp.arange(heads)[:, None]
    q_wide = jnp.where(owner[None], q_rot.reshape(count, 1, width), jnp.zeros((), BF16))
    scores = jnp.einsum("shc,sic->shi", q_wide, keys, preferred_element_type=F32)
    offset = lengths % BLK
    slots = jnp.arange(BLK, dtype=jnp.int32)
    lag = jnp.maximum(offset[:, None] - slots[None, :], 0).astype(F32)
    live = (slots[None, :] < offset[:, None])[:, None, :]
    factor = jnp.where(live, jnp.exp(-rate[None, :, None] * lag[:, None, :]), 0.0)
    weights = (scores * factor).astype(BF16)
    own = jnp.einsum("shn,shn->sh", q_rot, k_rot, preferred_element_type=F32).astype(BF16)
    inner = jnp.einsum("shi,sic->shc", weights, values, preferred_element_type=F32)
    carried = jnp.exp(-rate[None, :] * (offset[:, None] + 1).astype(F32))
    cross = jnp.einsum(
        "shk,skc->shc", q_rot, state.astype(BF16), preferred_element_type=F32
    )
    both = jnp.sum(jnp.where(owner[None], inner + cross * carried[..., None], 0.0), 1)
    retained = both.reshape(count, heads, HDIM) + own.astype(F32)[..., None] * v_new
    mean = jnp.mean(retained, -1, keepdims=True)
    centred = retained - mean
    spread = jnp.mean(centred * centred, -1, keepdims=True)
    normed = centred * lax.rsqrt(spread + EPS) * gain.reshape(heads, HDIM)[None]
    gate_f = jax.nn.silu(gated.astype(F32).reshape(count, heads, HDIM))
    return (gate_f * normed).reshape(count, heads * HDIM).astype(BF16)


def per_device(
    tokens,
    lengths,
    state_block,
    cached_keys,
    cached_values,
    query_weight,
    key_weight,
    value_weight,
    gate_weight,
    decay_rate,
    head_gain,
    out_weight,
    mixer_gain,
    up_weight,
    down_weight,
    final_gain,
):
    width = query_weight.shape[1]
    summed = project(tokens, query_weight, key_weight, value_weight, gate_weight)
    query, keyed, valued, gated = [
        summed[:, index * width : (index + 1) * width] for index in range(4)
    ]
    mixed = retain(
        query,
        keyed,
        valued,
        gated,
        lengths,
        state_block,
        cached_keys,
        cached_values,
        decay_rate,
        head_gain,
    )
    return mixer(mixed, tokens, out_weight, mixer_gain, up_weight, down_weight, final_gain)


def solution(mesh):
    return jax.shard_map(
        per_device,
        mesh=mesh,
        in_specs=(
            P("tp", "kv"),
            P("kv"),
            P("kv", None, "tp"),
            P("kv", None, "tp"),
            P("kv", None, "tp"),
            P("kv", "tp"),
            P("kv", "tp"),
            P("kv", "tp"),
            P("kv", "tp"),
            P("tp"),
            P("tp"),
            P("tp", "kv"),
            P("kv"),
            P("kv", "tp"),
            P("tp", "kv"),
            P("kv"),
        ),
        out_specs=P("tp", "kv"),
        check_vma=False,
    )
```

time: 273 us -> 118 us (0.43)
  waiting for transfers between devices: 139 us -> 0 us
  Pallas kernels: 0 us -> 101 us
  blocking collectives: 60 us -> 0 us
  local copies, waits for them, and re-layouts: 25.8 us -> 2.94 us
  matrix products: 21.4 us -> 7.8 us
  between operations: 13.4 us -> 0.16 us
  other arithmetic: 12 us -> 3.84 us
    pallas_call x0 -> x2, Pallas kernels: none -> 101 us  [the longest x1 76.7 us: mixer(): pl.pallas_call(mixer_kernel, name='mixer', out_shape=jax.ShapeDtypeStruct...]
    psum x1 -> x0, waiting for transfers between devices: 66 us -> none  [per_device(): lax.psum(jnp.dot(hidden_all, up_weight, preferred_element_type=jnp.float3...]
    reduce_scatter x2 -> x0, waiting for transfers between devices: 65.4 us -> none  [the longest x1 32.7 us: per_device(): lax.psum_scatter(jnp.dot(piece, down_weight, preferred_element_type=jnp.f...]
    all_gather x3 -> x0, blocking collectives: 40.2 us -> none  [the longest x1 16.8 us: per_device(): all_rows = lax.all_gather(tokens, 'tp', axis=0, tiled=True)]
    psum x2 -> x0, blocking collectives: 19.7 us -> none  [normalize(): lax.psum((jnp.sum(values, 1), jnp.sum(values * values, 1)), 'kv')]
    unnamed x23 -> x7, local copies, waits for them, and re-layouts: 17.2 us -> 1.48 us
    dot_general x9 -> x2, matrix products: 21.4 us -> 7.8 us  [the longest x1 5.2 us: retain(): jnp.einsum('shi,sic->shc', weights, values, preferred_element_type=F32)]
    unnamed x5 -> x0, waiting for transfers between devices: 7.78 us -> none
  transfers between devices with their start and end apart: 4 -> 0, of which waited for: 4 -> 0; matrix products, arithmetic and copies ran while one was open for 8% -> 0% of each run, Pallas kernels for 0% -> 0%
where the time goes in v1:
time: 118 us; the launch traced here: 116 us
  Pallas kernels  101 us (86%)
  matrix products  7.8 us (7%)
  other arithmetic  3.84 us (3%)
  local copies, waits for them, and re-layouts  2.94 us (2%)
    pallas_call x1, Pallas kernels, mixer(): pl.pallas_call(mixer_kernel, name='mixer', out_shape=jax.ShapeDtypeStruct...  76.7 us
    pallas_call x1, Pallas kernels, project(): pl.pallas_call(project_kernel, name='project', out_shape=jax.ShapeDtypeSt...  24.6 us
    dot_general x1, matrix products, retain(): jnp.einsum('shi,sic->shc', weights, values, preferred_element_type=F32)  5.2 us
    dot_general x1, matrix products, retain(): jnp.einsum('shk,skc->shc', q_rot, state.astype(BF16), preferred_element_t...  2.6 us

profile of v1, /device:TPU:0, one launch (start us, length us, event | category | flops | bytes accessed | tf_op | source)
XLA Modules:
  0.0 116.1 jit_solution(8238795509747072867)
XLA Ops:
  0.0 0.7 add_convert_fusion
  0.8 0.2 multiply_cosine_fusion
  1.0 24.6 %project.1 = bf16[64,1024]{1,0:T(8,128)(2,1)} custom-call(bf16[32,1024]{1,0:T(8,128)(2,1)} %tokens.3, bf16[1024,256]{1,0:T(8,128)(2,1)} %refs_0_.1, bf16[1024,256]{1,0:T(8,128)(2,1)} %refs_1_.1, bf16[1024,256]{1,0:T(8,128)(2,1)} %refs_2_.1, bf16[1024,256]{1,0:T(8,128)(2,1)} %refs_3_.1), custom_call_target="tpu_custom_call" | custom-call | tf_op jit(solution)/shard_map/project/pallas_call | solution.py:120
  25.6 0.8 slice_convert_fusion
  26.4 0.1 reshape.230
  26.5 0.2 multiply_subtract_fusion
  26.7 0.1 reshape.228
  26.8 0.2 multiply_subtract_fusion.1
  27.0 0.3 fusion.17
  27.6 5.2 %fusion.15 = f32[64,4,256]{2,1,0:T(4,128)S(1)} fusion(bf16[64,128,256]{2,1,0:T(8,128)(2,1)} %param.20, bf16[64,128,256]{2,1,0:T(8,128)(2,1)} %param.19, pred[4,256]{1,0:T(4,128)(4,1)S(1)} %iota_compare_fusion.1, f32[64,128]{1,0:T(8,128)S(1)} %maximum_convert_fusion.1, f32[4]{0:T(128)S(1)} %neg.21, bf16[64,256]{1,0:T(8,128)(2,1)S(1)} %convert_element_type.54, ...), kind=kOutput, calls=%fused_computation.8 | convolution fusion | flops 33751040 | bytes 8725520 | tf_op jit(solution)/shard_map/shi,sic->shc/dot_general | solution.py:327
  33.0 2.6 %fusion.11 = f32[64,256]{1,0:T(8,128)S(1)} fusion(f32[64,4,256]{2,1,0:T(4,128)S(1)} %fusion.15, bf16[64,4,64]{2,1,0:T(4,128)(2,1)S(1)} %get-tuple-element.6, f32[64,64,256]{2,1,0:T(8,128)} %param.18, f32[64,4]{1,0:T(8,128)S(1)} %copy.17, pred[4,256]{1,0:T(4,128)(4,1)S(1)} %iota_compare_fusion.1), kind=kOutput, calls=%fused_computation.5 | convolution fusion | flops 9682944 | bytes 4556800 | tf_op jit(solution)/shard_map/shk,skc->shc/dot_general | solution.py:329
  35.6 0.1 reshape.225
  35.7 0.1 reshape.226
  35.8 0.2 fusion.38
  36.1 0.3 multiply_reduce_fusion
  36.4 0.1 mul.201
  36.5 0.1 mul.202
  36.7 0.1 sub.44
  36.8 0.1 sub.45
  36.9 0.1 mul.196
  37.1 0.1 mul.197
  37.2 0.7 fusion.36.mixed
  37.9 76.7 %mixer.1 = bf16[32,1024]{1,0:T(8,128)(2,1)} custom-call(bf16[64,256]{1,0:T(8,128)(2,1)} %fusion.36.mixed, bf16[32,1024]{1,0:T(8,128)(2,1)} %tokens.3, bf16[256,1024]{1,0:T(8,128)(2,1)} %out_w.1, f32[1,1024]{1,0:T(1,128)} %bitcast.5, bf16[1024,2048]{1,0:T(8,128)(2,1)} %up_w.1, bf16[2048,1024]{1,0:T(8,128)(2,1)} %down_w.1, f32[1,1024]{1,0:T(1,128)} %bitcast.6), custom_call_target="tpu_custom_call" | custom-call | tf_op jit(solution)/shard_map/mixer/pallas_call | solution.py:264
  114.6 1.5 %copy.24 = bf16[32,1024]{1,0:T(8,128)(2,1)} copy(bf16[32,1024]{1,0:T(8,128)(2,1)} %mixer.1) | data formatting | bytes 131072
  (18 shorter events, 0.5 us)
Async XLA Ops:
  0.0 27.6 %copy-start.2 = (f32[4]{0:T(128)S(1)}, f32[4]{0:T(128)}, u32[]{:S(2)}) copy-start(f32[4]{0:T(128)} %param.25) | copy-start | bytes 52
  32.8 4.4 %copy-start = (bf16[64,1024]{1,0:T(8,128)(2,1)S(1)}, bf16[64,1024]{1,0:T(8,128)(2,1)}, u32[]{:S(2)}) copy-start(bf16[64,1024]{1,0:T(8,128)(2,1)} %project.1) | copy-start | bytes 393220
  32.8 4.4 %copy-start.1 = (f32[256]{0:T(256)S(1)}, f32[256]{0:T(256)}, u32[]{:S(2)}) copy-start(f32[256]{0:T(256)} %param.26) | copy-start | bytes 3076

commit v2 on v1

--- a/solution.py
+++ b/solution.py
@@ -78,6 +78,101 @@
         return self.own[...].astype(F32) + jnp.sum(self.landed[...].astype(F32), 0)
 
 
+PAIR = 2
+
+
+def chip():
+    me = lax.axis_index("tp")
+    return me // PAIR, lax.rem(me, PAIR), lax.axis_size("tp") // PAIR
+
+
+def to_tp(target, src, dst, sems, index):
+    return pltpu.make_async_remote_copy(
+        src_ref=src,
+        dst_ref=dst,
+        send_sem=sems.at[0, index],
+        recv_sem=sems.at[1, index],
+        device_id={"tp": target},
+        device_id_type=MESH,
+    )
+
+
+class ChipGather:
+    def __init__(self, src, held, sems):
+        z, core, chips = chip()
+        me, other = z * PAIR + core, z * PAIR + 1 - core
+        self.first = [to_tp(other, src, held.at[me], sems, 0)]
+        self.handed = []
+        for step in range(1, chips):
+            target = lax.rem(z + step, chips) * PAIR + core
+            self.first.append(to_tp(target, src, held.at[me], sems, step))
+            owner = lax.rem(z + chips - step, chips) * PAIR + core
+            block = held.at[owner]
+            self.handed.append(to_tp(other, block, block, sems, chips + step - 1))
+
+    def start(self):
+        for copy in self.first[1:] + self.first[:1]:
+            copy.start()
+
+    def wait_recv(self):
+        for copy, handed in zip(self.first[1:], self.handed):
+            copy.wait_recv()
+            handed.start()
+        self.first[0].wait_recv()
+        for handed in self.handed:
+            handed.wait_recv()
+
+    def wait_send(self):
+        for copy in self.first + self.handed:
+            copy.wait_send()
+
+
+class ChipScatter:
+    def __init__(self, parts, from_pair, sums, landed, sems):
+        z, core, chips = chip()
+        other = z * PAIR + 1 - core
+        self.parts, self.from_pair, self.sums, self.landed = parts, from_pair, sums, landed
+        self.pair, self.far = [], []
+        for step in list(range(1, chips)) + [0]:
+            there = lax.rem(z + step, chips)
+            self.pair.append(
+                to_tp(other, parts.at[1 - core, there], from_pair.at[there], sems, step)
+            )
+            if step:
+                self.far.append(
+                    to_tp(
+                        there * PAIR + core, sums.at[step - 1], landed.at[step - 1], sems,
+                        chips + step - 1,
+                    )
+                )
+
+    def fill(self, part):
+        _, _, chips = chip()
+        split = part.astype(BF16).reshape(chips, PAIR, *self.landed.shape[1:])
+        for core in range(PAIR):
+            self.parts[core] = split[:, core]
+
+    def total(self):
+        z, core, chips = chip()
+        for copy in self.pair:
+            copy.start()
+        for step in range(1, chips):
+            there = lax.rem(z + step, chips)
+            self.pair[step - 1].wait_recv()
+            both = self.parts[core, there].astype(F32) + self.from_pair[there].astype(F32)
+            self.sums[step - 1] = both.astype(BF16)
+            self.far[step - 1].start()
+        self.pair[chips - 1].wait_recv()
+        both = self.parts[core, z].astype(F32) + self.from_pair[z].astype(F32)
+        for copy in self.far:
+            copy.wait_recv()
+        return both + jnp.sum(self.landed[...].astype(F32), 0)
+
+    def wait_send(self):
+        for copy in self.pair + self.far:
+            copy.wait_send()
+
+
 def project_kernel(tokens, *refs):
     weights, (out, rows, held, parts, landed, tok_sems, part_sems, load_sems) = refs[:4], refs[4:]
     loads = [
@@ -87,7 +182,7 @@
     for load in loads:
         load.start()
     enter(("tp", "kv"))
-    gather = Gather("tp", tokens, rows, tok_sems)
+    gather = ChipGather(tokens, rows, tok_sems)
     gather.start()
     rows[lax.axis_index("tp")] = tokens[...]
     gather.wait_recv()
@@ -166,7 +261,7 @@
 
 def mixer_kernel(
     mixed, tokens, out_w, mixer_gain, up_w, down_w, final_gain, out,
-    out_v, up_v, down_v, heads, branch_parts, branch_landed, stat_mine, stat_landed,
+    out_v, up_v, down_v, heads, branch_parts, pair_landed, pair_sums, branch_landed, stat_mine, stat_landed,
     hidden_mine, hidden_all, up_parts, up_landed, act_mine, act_all, down_sum,
     load_sems, mix_sems, branch_sems, stat_sems, hid_sems, up_sems, act_sems, down_sems,
 ):
@@ -186,14 +281,14 @@
     loads[0].wait()
     gather.wait_recv()
     part = jnp.dot(heads[...].reshape(nkv * seqs, width), out_v[...], preferred_element_type=F32)
-    branch_parts[0] = part.astype(BF16).reshape(ntp, block, depth)
-    branch = Scatter("tp", branch_parts.at[0], branch_landed.at[0], branch_sems)
-    branch.start()
-    branch.wait_recv()
+    branch = ChipScatter(
+        branch_parts.at[0], pair_landed.at[0], pair_sums.at[0], branch_landed.at[0], branch_sems
+    )
+    branch.fill(part)
     values = ALPHA * tokens[...].astype(F32) + branch.total()
     hidden = normalize(values, mixer_gain, stat_mine.at[0], stat_landed.at[0], stat_sems.at[0])
     hidden_mine[...] = hidden.astype(BF16)
-    spread = Gather("tp", hidden_mine, hidden_all, hid_sems)
+    spread = ChipGather(hidden_mine, hidden_all, hid_sems)
     spread.start()
     hidden_all[tp] = hidden_mine[...]
     loads[1].wait()
@@ -236,10 +331,10 @@
             preferred_element_type=F32,
         )
 
-    branch_parts[1] = down_sum[...].astype(BF16).reshape(ntp, block, depth)
-    downward = Scatter("tp", branch_parts.at[1], branch_landed.at[1], down_sems)
-    downward.start()
-    downward.wait_recv()
+    downward = ChipScatter(
+        branch_parts.at[1], pair_landed.at[1], pair_sums.at[1], branch_landed.at[1], down_sems
+    )
+    downward.fill(down_sum[...])
     values = ALPHA * hidden_mine[...].astype(F32) + downward.total()
     result = normalize(values, final_gain, stat_mine.at[1], stat_landed.at[1], stat_sems.at[1])
     out[...] = result.astype(BF16)
@@ -257,6 +352,7 @@
     seqs, width = mixed.shape
     block, depth = tokens.shape
     inner = up_w.shape[1]
+    chips = ntp // PAIR
     tile = min(TILE, inner)
     tiles = inner // tile
     vmem, anyw = pl.BlockSpec(memory_space=pltpu.VMEM), pl.BlockSpec(memory_space=pl.ANY)
@@ -272,8 +368,10 @@
             pltpu.VMEM((depth, inner), BF16),
             pltpu.VMEM((inner, depth), BF16),
             pltpu.VMEM((nkv, seqs, width), BF16),
-            pltpu.VMEM((2, ntp, block, depth), BF16),
-            pltpu.VMEM((2, ntp - 1, block, depth), BF16),
+            pltpu.VMEM((2, PAIR, chips, block, depth), BF16),
+            pltpu.VMEM((2, chips, block, depth), BF16),
+            pltpu.VMEM((2, chips - 1, block, depth), BF16),
+            pltpu.VMEM((2, chips - 1, block, depth), BF16),
             pltpu.VMEM((2, block, 128), F32),
             pltpu.VMEM((2, nkv - 1, block, 128), F32),
             pltpu.VMEM((block, depth), BF16),

time: 118 us -> 103 us (0.87); the launches traced: 116 us -> 103 us
  Pallas kernels: 101 us -> 87.8 us
    pallas_call x1, Pallas kernels: 76.7 us -> 64.9 us  [mixer(): pl.pallas_call(mixer_kernel, name='mixer', out_shape=jax.ShapeDtypeStruct...]
    pallas_call x1, Pallas kernels: 24.6 us -> 22.8 us  [project(): pl.pallas_call(project_kernel, name='project', out_shape=jax.ShapeDtypeSt...]
where the time goes in v2:
time: 103 us
  Pallas kernels  87.8 us (85%)
  matrix products  7.8 us (8%)
  other arithmetic  3.84 us (4%)
  local copies, waits for them, and re-layouts  2.94 us (3%)
    pallas_call x1, Pallas kernels, mixer(): pl.pallas_call(mixer_kernel, name='mixer', out_shape=jax.ShapeDtypeStruct...  64.9 us
    pallas_call x1, Pallas kernels, project(): pl.pallas_call(project_kernel, name='project', out_shape=jax.ShapeDtypeSt...  22.8 us
    dot_general x1, matrix products, retain(): jnp.einsum('shi,sic->shc', weights, values, preferred_element_type=F32)  5.2 us
    dot_general x1, matrix products, retain(): jnp.einsum('shk,skc->shc', q_rot, state.astype(BF16), preferred_element_t...  2.6 us

profile of v2, /device:TPU:0, one launch (start us, length us, event | category | flops | bytes accessed | tf_op | source)
XLA Modules:
  0.0 102.5 jit_solution(3002683663571373086)
XLA Ops:
  0.0 0.7 add_convert_fusion
  0.8 0.2 multiply_cosine_fusion
  1.0 22.8 %project.1 = bf16[64,1024]{1,0:T(8,128)(2,1)} custom-call(bf16[32,1024]{1,0:T(8,128)(2,1)} %tokens.3, bf16[1024,256]{1,0:T(8,128)(2,1)} %refs_0_.1, bf16[1024,256]{1,0:T(8,128)(2,1)} %refs_1_.1, bf16[1024,256]{1,0:T(8,128)(2,1)} %refs_2_.1, bf16[1024,256]{1,0:T(8,128)(2,1)} %refs_3_.1), custom_call_target="tpu_custom_call" | custom-call | tf_op jit(solution)/shard_map/project/pallas_call | solution.py:215
  23.8 0.8 slice_convert_fusion
  24.6 0.1 reshape.230
  24.7 0.2 multiply_subtract_fusion
  24.9 0.1 reshape.228
  25.0 0.2 multiply_subtract_fusion.1
  25.2 0.3 fusion.17
  25.8 5.2 %fusion.15 = f32[64,4,256]{2,1,0:T(4,128)S(1)} fusion(bf16[64,128,256]{2,1,0:T(8,128)(2,1)} %param.20, bf16[64,128,256]{2,1,0:T(8,128)(2,1)} %param.19, pred[4,256]{1,0:T(4,128)(4,1)S(1)} %iota_compare_fusion.1, f32[64,128]{1,0:T(8,128)S(1)} %maximum_convert_fusion.1, f32[4]{0:T(128)S(1)} %neg.21, bf16[64,256]{1,0:T(8,128)(2,1)S(1)} %convert_element_type.54, ...), kind=kOutput, calls=%fused_computation.8 | convolution fusion | flops 33751040 | bytes 8725520 | tf_op jit(solution)/shard_map/shi,sic->shc/dot_general | solution.py:425
  31.2 2.6 %fusion.11 = f32[64,256]{1,0:T(8,128)S(1)} fusion(f32[64,4,256]{2,1,0:T(4,128)S(1)} %fusion.15, bf16[64,4,64]{2,1,0:T(4,128)(2,1)S(1)} %get-tuple-element.6, f32[64,64,256]{2,1,0:T(8,128)} %param.18, f32[64,4]{1,0:T(8,128)S(1)} %copy.17, pred[4,256]{1,0:T(4,128)(4,1)S(1)} %iota_compare_fusion.1), kind=kOutput, calls=%fused_computation.5 | convolution fusion | flops 9682944 | bytes 4556800 | tf_op jit(solution)/shard_map/shk,skc->shc/dot_general | solution.py:427
  33.8 0.1 reshape.225
  33.9 0.1 reshape.226
  34.1 0.2 fusion.38
  34.3 0.3 multiply_reduce_fusion
  34.6 0.1 mul.201
  34.7 0.1 mul.202
  34.9 0.1 sub.44
  35.0 0.1 sub.45
  35.2 0.1 mul.196
  35.3 0.1 mul.197
  35.4 0.7 fusion.36.mixed
  36.1 64.9 %mixer.1 = bf16[32,1024]{1,0:T(8,128)(2,1)} custom-call(bf16[64,256]{1,0:T(8,128)(2,1)} %fusion.36.mixed, bf16[32,1024]{1,0:T(8,128)(2,1)} %tokens.3, bf16[256,1024]{1,0:T(8,128)(2,1)} %out_w.1, f32[1,1024]{1,0:T(1,128)} %bitcast.5, bf16[1024,2048]{1,0:T(8,128)(2,1)} %up_w.1, bf16[2048,1024]{1,0:T(8,128)(2,1)} %down_w.1, f32[1,1024]{1,0:T(1,128)} %bitcast.6), custom_call_target="tpu_custom_call" | custom-call | tf_op jit(solution)/shard_map/mixer/pallas_call | solution.py:360
  101.0 1.5 %copy.24 = bf16[32,1024]{1,0:T(8,128)(2,1)} copy(bf16[32,1024]{1,0:T(8,128)(2,1)} %mixer.1) | data formatting | bytes 131072
  (18 shorter events, 0.5 us)
Async XLA Ops:
  0.0 25.8 %copy-start.2 = (f32[4]{0:T(128)S(1)}, f32[4]{0:T(128)}, u32[]{:S(2)}) copy-start(f32[4]{0:T(128)} %param.25) | copy-start | bytes 52
  31.0 4.4 %copy-start = (bf16[64,1024]{1,0:T(8,128)(2,1)S(1)}, bf16[64,1024]{1,0:T(8,128)(2,1)}, u32[]{:S(2)}) copy-start(bf16[64,1024]{1,0:T(8,128)(2,1)} %project.1) | copy-start | bytes 393220
  31.0 4.4 %copy-start.1 = (f32[256]{0:T(256)S(1)}, f32[256]{0:T(256)}, u32[]{:S(2)}) copy-start(f32[256]{0:T(256)} %param.26) | copy-start | bytes 3076

commit v3 on v2

--- a/solution.py
+++ b/solution.py
@@ -1,3 +1,5 @@
+import math
+
 import jax
 import jax.numpy as jnp
 from jax import lax
@@ -262,8 +264,8 @@
 def mixer_kernel(
     mixed, tokens, out_w, mixer_gain, up_w, down_w, final_gain, out,
     out_v, up_v, down_v, heads, branch_parts, pair_landed, pair_sums, branch_landed, stat_mine, stat_landed,
-    hidden_mine, hidden_all, up_parts, up_landed, act_mine, act_all, down_sum,
-    load_sems, mix_sems, branch_sems, stat_sems, hid_sems, up_sems, act_sems, down_sems,
+    hidden_mine, hidden_all, up_parts, up_landed, up_sums, up_final, act_mine, act_all, down_sum,
+    load_sems, mix_sems, branch_sems, stat_sems, hid_sems, up_sems, down_sems,
 ):
     loads = [
         pltpu.make_async_copy(src, dst, load_sems.at[index])
@@ -293,43 +295,124 @@
     hidden_all[tp] = hidden_mine[...]
     loads[1].wait()
     spread.wait_recv()
-    tiles, tile = up_parts.shape[0], up_parts.shape[3]
-
-    def up_scatter(index):
-        return Scatter("kv", up_parts.at[index], up_landed.at[index], up_sems.at[index])
-
-    def act_gather(index):
-        return Gather("kv", act_mine.at[index], act_all.at[index], act_sems.at[index])
-
-    @pl.loop(0, tiles)
-    def _(index):
+    tiles, tile = up_parts.shape[0], up_parts.shape[4]
+
+    side = up_parts.shape[1]
+    here = (kv // side, lax.rem(kv, side))
+
+    def neighbour(axis, step):
+        there = lax.rem(here[axis] + step, side)
+        target = there * side + here[1] if axis == 0 else here[0] * side + there
+        return there, target
+
+    def to_kv(target, src, dst, index, stage, step):
+        return pltpu.make_async_remote_copy(
+            src_ref=src,
+            dst_ref=dst,
+            send_sem=up_sems.at[index, 0, stage, step],
+            recv_sem=up_sems.at[index, 1, stage, step],
+            device_id={"kv": target},
+            device_id_type=MESH,
+        )
+
+    def first_sums(index, axis):
+        copies = []
+        for step in range(1, side):
+            there, target = neighbour(axis, step)
+            copies.append(
+                to_kv(target, up_parts.at[index, there], up_landed.at[index, step - 1], index, 0, step)
+            )
+        return copies
+
+    def second_sums(index, axis):
+        copies = []
+        for step in range(1, side):
+            there, target = neighbour(1 - axis, step)
+            copies.append(
+                to_kv(target, up_sums.at[index, there], up_final.at[index, step - 1], index, 1, step)
+            )
+        return copies
+
+    def first_spread(index, axis):
+        return [
+            to_kv(neighbour(1 - axis, step)[1], act_mine.at[index], act_all.at[index, kv], index, 2, step)
+            for step in range(1, side)
+        ]
+
+    def second_spread(index, axis):
+        copies = []
+        for far in range(side):
+            line = lax.rem(here[1 - axis] + side - far, side)
+            owner = line * side + here[1] if axis == 1 else here[0] * side + line
+            block = act_all.at[index, owner] if far else act_mine.at[index]
+            for step in range(1, side):
+                target = neighbour(axis, step)[1]
+                copies.append(
+                    to_kv(target, block, act_all.at[index, owner], index, 3 + far, step)
+                )
+        return copies
+
+    def each_tile(body):
+        @pl.loop(0, tiles // 2)
+        def _(half):
+            for axis in (1, 0):
+                body(2 * half + (1 - axis), axis)
+
+    def start(copies):
+        for copy in copies:
+            copy.start()
+
+    def arrive(copies):
+        for copy in copies:
+            copy.wait_recv()
+
+    def multiply_up(index, axis):
         columns = pl.ds(pl.multiple_of(index * tile, tile), tile)
         part = jnp.dot(
             hidden_all[...].reshape(ntp * block, depth), up_v[:, columns],
             preferred_element_type=F32,
         )
-        up_parts[index] = part.astype(BF16).reshape(nkv, seqs, tile)
-        up_scatter(index).start()
-
-    @pl.loop(0, tiles)
-    def _(index):
-        send = up_scatter(index)
-        send.wait_recv()
-        act_mine[index] = jnp.square(jnp.maximum(send.total(), 0.0)).astype(BF16)
-        act_gather(index).start()
+        part = part.astype(BF16).reshape(side, side, seqs, tile)
+        if axis == 0:
+            up_parts[index] = part
+        else:
+            for column in range(side):
+                up_parts[index, column] = part[:, column]
+        start(first_sums(index, axis))
+
+    def add_first(index, axis):
+        arrive(first_sums(index, axis))
+        both = up_parts[index, here[axis]].astype(F32)
+        both = both + jnp.sum(up_landed[index].astype(F32), 0)
+        up_sums[index] = both.astype(BF16)
+        start(second_sums(index, axis))
+
+    def add_second(index, axis):
+        arrive(second_sums(index, axis))
+        both = up_sums[index, here[1 - axis]].astype(F32)
+        both = both + jnp.sum(up_final[index].astype(F32), 0)
+        act_mine[index] = jnp.square(jnp.maximum(both, 0.0)).astype(BF16)
+        start(first_spread(index, axis))
+        start(second_spread(index, axis)[: side - 1])
         act_all[index, kv] = act_mine[index]
+
+    def hand_on(index, axis):
+        arrive(first_spread(index, axis))
+        start(second_spread(index, axis)[side - 1 :])
 
     loads[2].wait()
     down_sum[...] = jnp.zeros_like(down_sum)
 
-    @pl.loop(0, tiles)
-    def _(index):
-        act_gather(index).wait_recv()
+    def multiply_down(index, axis):
+        arrive(second_spread(index, axis))
         down_sum[...] += jnp.dot(
             act_all[index].reshape(nkv * seqs, tile),
             down_v[pl.ds(pl.multiple_of(index * tile, tile), tile), :],
             preferred_element_type=F32,
         )
+
+    for body in (multiply_up, add_first, add_second, hand_on, multiply_down):
+        each_tile(body)
 
     downward = ChipScatter(
         branch_parts.at[1], pair_landed.at[1], pair_sums.at[1], branch_landed.at[1], down_sems
@@ -341,10 +424,12 @@
     for group in (gather, branch, spread, downward):
         group.wait_send()
 
-    @pl.loop(0, tiles)
-    def _(index):
-        up_scatter(index).wait_send()
-        act_gather(index).wait_send()
+    def wait_sends(index, axis):
+        for group in (first_sums, second_sums, first_spread, second_spread):
+            for copy in group(index, axis):
+                copy.wait_send()
+
+    each_tile(wait_sends)
 
 
 def mixer(mixed, tokens, out_w, mixer_gain, up_w, down_w, final_gain):
@@ -353,6 +438,7 @@
     block, depth = tokens.shape
     inner = up_w.shape[1]
     chips = ntp // PAIR
+    side = math.isqrt(nkv)
     tile = min(TILE, inner)
     tiles = inner // tile
     vmem, anyw = pl.BlockSpec(memory_space=pltpu.VMEM), pl.BlockSpec(memory_space=pl.ANY)
@@ -376,8 +462,10 @@
             pltpu.VMEM((2, nkv - 1, block, 128), F32),
             pltpu.VMEM((block, depth), BF16),
             pltpu.VMEM((ntp, block, depth), BF16),
-            pltpu.VMEM((tiles, nkv, seqs, tile), BF16),
-            pltpu.VMEM((tiles, nkv - 1, seqs, tile), BF16),
+            pltpu.VMEM((tiles, side, side, seqs, tile), BF16),
+            pltpu.VMEM((tiles, side - 1, side, seqs, tile), BF16),
+            pltpu.VMEM((tiles, side, seqs, tile), BF16),
+            pltpu.VMEM((tiles, side - 1, seqs, tile), BF16),
             pltpu.VMEM((tiles, seqs, tile), BF16),
             pltpu.VMEM((tiles, nkv, seqs, tile), BF16),
             pltpu.VMEM((ntp * block, depth), F32),
@@ -386,8 +474,7 @@
             dma((2, ntp - 1)),
             dma((2, 2, nkv - 1)),
             dma((2, ntp - 1)),
-            dma((tiles, 2, nkv - 1)),
-            dma((tiles, 2, nkv - 1)),
+            dma((tiles, 2, side + 3, side)),
             dma((2, ntp - 1)),
         ],
         compiler_params=pltpu.CompilerParams(

time: 103 us -> 98.6 us (0.957)
  Pallas kernels: 87.8 us -> 83.5 us
    pallas_call x1, Pallas kernels: 64.9 us -> 60.7 us  [mixer(): pl.pallas_call(mixer_kernel, name='mixer', out_shape=jax.ShapeDtypeStruct...]
where the time goes in v3:
time: 98.6 us; the launch traced here: 98.2 us
  Pallas kernels  83.5 us (85%)
  matrix products  7.8 us (8%)
  other arithmetic  3.84 us (4%)
  local copies, waits for them, and re-layouts  2.94 us (3%)
    pallas_call x1, Pallas kernels, mixer(): pl.pallas_call(mixer_kernel, name='mixer', out_shape=jax.ShapeDtypeStruct...  60.7 us
    pallas_call x1, Pallas kernels, project(): pl.pallas_call(project_kernel, name='project', out_shape=jax.ShapeDtypeSt...  22.8 us
    dot_general x1, matrix products, retain(): jnp.einsum('shi,sic->shc', weights, values, preferred_element_type=F32)  5.2 us
    dot_general x1, matrix products, retain(): jnp.einsum('shk,skc->shc', q_rot, state.astype(BF16), preferred_element_t...  2.6 us

profile of v3, /device:TPU:0, one launch (start us, length us, event | category | flops | bytes accessed | tf_op | source)
XLA Modules:
  0.0 98.2 jit_solution(9184110365280139093)
XLA Ops:
  0.0 0.7 add_convert_fusion
  0.8 0.2 multiply_cosine_fusion
  1.0 22.8 %project.1 = bf16[64,1024]{1,0:T(8,128)(2,1)} custom-call(bf16[32,1024]{1,0:T(8,128)(2,1)} %tokens.3, bf16[1024,256]{1,0:T(8,128)(2,1)} %refs_0_.1, bf16[1024,256]{1,0:T(8,128)(2,1)} %refs_1_.1, bf16[1024,256]{1,0:T(8,128)(2,1)} %refs_2_.1, bf16[1024,256]{1,0:T(8,128)(2,1)} %refs_3_.1), custom_call_target="tpu_custom_call" | custom-call | tf_op jit(solution)/shard_map/project/pallas_call | solution.py:217
  23.8 0.8 slice_convert_fusion
  24.6 0.1 reshape.230
  24.7 0.2 multiply_subtract_fusion
  24.9 0.1 reshape.228
  25.0 0.2 multiply_subtract_fusion.1
  25.2 0.3 fusion.17
  25.8 5.2 %fusion.15 = f32[64,4,256]{2,1,0:T(4,128)S(1)} fusion(bf16[64,128,256]{2,1,0:T(8,128)(2,1)} %param.20, bf16[64,128,256]{2,1,0:T(8,128)(2,1)} %param.19, pred[4,256]{1,0:T(4,128)(4,1)S(1)} %iota_compare_fusion.1, f32[64,128]{1,0:T(8,128)S(1)} %maximum_convert_fusion.1, f32[4]{0:T(128)S(1)} %neg.21, bf16[64,256]{1,0:T(8,128)(2,1)S(1)} %convert_element_type.54, ...), kind=kOutput, calls=%fused_computation.8 | convolution fusion | flops 33751040 | bytes 8725520 | tf_op jit(solution)/shard_map/shi,sic->shc/dot_general | solution.py:512
  31.2 2.6 %fusion.11 = f32[64,256]{1,0:T(8,128)S(1)} fusion(f32[64,4,256]{2,1,0:T(4,128)S(1)} %fusion.15, bf16[64,4,64]{2,1,0:T(4,128)(2,1)S(1)} %get-tuple-element.6, f32[64,64,256]{2,1,0:T(8,128)} %param.18, f32[64,4]{1,0:T(8,128)S(1)} %copy.17, pred[4,256]{1,0:T(4,128)(4,1)S(1)} %iota_compare_fusion.1), kind=kOutput, calls=%fused_computation.5 | convolution fusion | flops 9682944 | bytes 4556800 | tf_op jit(solution)/shard_map/shk,skc->shc/dot_general | solution.py:514
  33.8 0.1 reshape.225
  33.9 0.1 reshape.226
  34.1 0.2 fusion.38
  34.3 0.3 multiply_reduce_fusion
  34.6 0.1 mul.201
  34.7 0.1 mul.202
  34.9 0.1 sub.44
  35.0 0.1 sub.45
  35.2 0.1 mul.196
  35.3 0.1 mul.197
  35.4 0.7 fusion.36.mixed
  36.1 60.7 %mixer.1 = bf16[32,1024]{1,0:T(8,128)(2,1)} custom-call(bf16[64,256]{1,0:T(8,128)(2,1)} %fusion.36.mixed, bf16[32,1024]{1,0:T(8,128)(2,1)} %tokens.3, bf16[256,1024]{1,0:T(8,128)(2,1)} %out_w.1, f32[1,1024]{1,0:T(1,128)} %bitcast.5, bf16[1024,2048]{1,0:T(8,128)(2,1)} %up_w.1, bf16[2048,1024]{1,0:T(8,128)(2,1)} %down_w.1, f32[1,1024]{1,0:T(1,128)} %bitcast.6), custom_call_target="tpu_custom_call" | custom-call | tf_op jit(solution)/shard_map/mixer/pallas_call | solution.py:446
  96.8 1.5 %copy.24 = bf16[32,1024]{1,0:T(8,128)(2,1)} copy(bf16[32,1024]{1,0:T(8,128)(2,1)} %mixer.1) | data formatting | bytes 131072
  (18 shorter events, 0.5 us)
Async XLA Ops:
  0.0 25.8 %copy-start.2 = (f32[4]{0:T(128)S(1)}, f32[4]{0:T(128)}, u32[]{:S(2)}) copy-start(f32[4]{0:T(128)} %param.25) | copy-start | bytes 52
  31.0 4.4 %copy-start = (bf16[64,1024]{1,0:T(8,128)(2,1)S(1)}, bf16[64,1024]{1,0:T(8,128)(2,1)}, u32[]{:S(2)}) copy-start(bf16[64,1024]{1,0:T(8,128)(2,1)} %project.1) | copy-start | bytes 393220
  31.0 4.4 %copy-start.1 = (f32[256]{0:T(256)S(1)}, f32[256]{0:T(256)}, u32[]{:S(2)}) copy-start(f32[256]{0:T(256)} %param.26) | copy-start | bytes 3076

commit v4 on v3

--- a/solution.py
+++ b/solution.py
@@ -10,6 +10,7 @@
 HDIM = 64
 BLK = 128
 TILE = 256
+HEAD_ROWS = 16
 
 ALPHA = 2.0**0.5
 EPS = 1e-05
@@ -175,13 +176,15 @@
             copy.wait_send()
 
 
-def project_kernel(tokens, *refs):
+def project_kernel(caches, tokens, *refs):
     weights, (out, rows, held, parts, landed, tok_sems, part_sems, load_sems) = refs[:4], refs[4:]
     loads = [
         pltpu.make_async_copy(weight, held.at[index], load_sems.at[index])
         for index, weight in enumerate(weights)
     ]
     for load in loads:
+        load.start()
+    for load in caches:
         load.start()
     enter(("tp", "kv"))
     gather = ChipGather(tokens, rows, tok_sems)
@@ -209,30 +212,68 @@
         send.wait_send()
 
 
-def project(tokens, *weights):
-    ntp, nkv = lax.axis_size("tp"), lax.axis_size("kv")
-    block, depth = tokens.shape
-    width = weights[0].shape[1]
-    seqs = block * ntp // nkv
-    return pl.pallas_call(
-        project_kernel,
-        name="project",
-        out_shape=jax.ShapeDtypeStruct((seqs, 4 * width), BF16),
-        in_specs=[pl.BlockSpec(memory_space=pltpu.VMEM)] + [pl.BlockSpec(memory_space=pl.ANY)] * 4,
-        out_specs=pl.BlockSpec(memory_space=pltpu.VMEM),
-        scratch_shapes=[
-            pltpu.VMEM((ntp, block, depth), BF16),
-            pltpu.VMEM((4, depth, width), BF16),
-            pltpu.VMEM((4, nkv, seqs, width), BF16),
-            pltpu.VMEM((4, nkv - 1, seqs, width), BF16),
-            pltpu.SemaphoreType.DMA((2, ntp - 1)),
-            pltpu.SemaphoreType.DMA((2, 4, nkv - 1)),
-            pltpu.SemaphoreType.DMA((4,)),
-        ],
-        compiler_params=pltpu.CompilerParams(
-            collective_id=0, has_side_effects=True, vmem_limit_bytes=60 * 2**20
-        ),
-    )(tokens, *weights)
+def load_caches(caches, held, sems):
+    return [
+        pltpu.make_async_copy(src, dst, sems.at[index])
+        for index, (src, dst) in enumerate(zip(caches, held))
+    ]
+
+
+def retain_kernel(summed, cos, sin, carried, factor, gain, mixed, keys, values, state, wide, kept):
+    seqs, width = mixed.shape
+    rows = wide.shape[1]
+    query, keyed, valued, gated = [
+        summed[:, index * width : (index + 1) * width] for index in range(4)
+    ]
+    above = lax.broadcasted_iota(jnp.int32, (width, width), 0)
+    across = lax.broadcasted_iota(jnp.int32, (width, width), 1)
+    half = HDIM // 2
+    first = across % HDIM < half
+    swap = jnp.where(first & (above == across + half), -1.0, 0.0)
+    swap = jnp.where(~first & (above == across - half), 1.0, swap).astype(BF16)
+    same = jnp.where(above // HDIM == across // HDIM, 1.0, 0.0)
+    tall = lax.broadcasted_iota(jnp.int32, (width, HDIM), 0)
+    narrow = lax.broadcasted_iota(jnp.int32, (width, HDIM), 1)
+    fold = jnp.where(tall % HDIM == narrow, 1.0, 0.0).astype(BF16)
+    head = lax.broadcasted_iota(jnp.int32, (rows, width), 0)
+    lane = lax.broadcasted_iota(jnp.int32, (rows, width), 1)
+    owner = jnp.where(lane // HDIM == head, 1.0, 0.0)
+
+    def rotate(vectors):
+        turned = jnp.dot(vectors, swap, preferred_element_type=F32)
+        return vectors.astype(F32) * cos[...] + turned * sin[...]
+
+    def per_head(terms):
+        return jnp.dot(
+            terms, same, preferred_element_type=F32, precision=lax.Precision.HIGHEST
+        )
+
+    q_rot = rotate(query).astype(BF16).astype(F32)
+    k_rot = (rotate(keyed) * 0.125).astype(BF16).astype(F32)
+    own = per_head(q_rot * k_rot).astype(BF16).astype(F32)
+    wide[...] = q_rot[:, None, :] * owner[None]
+    group = 8
+
+    @pl.loop(0, seqs // group)
+    def _(outer):
+        for inner in range(group):
+            index = outer * group + inner
+            spread = wide[index].astype(BF16)
+            scores = lax.dot_general(
+                spread, keys[index], (((1,), (1,)), ((), ())), preferred_element_type=F32
+            )
+            weights = (scores * factor[index]).astype(BF16)
+            within = jnp.dot(weights, values[index], preferred_element_type=F32)
+            short = jnp.dot(spread, fold, preferred_element_type=F32).astype(BF16)
+            cross = jnp.dot(short, state[index].astype(BF16), preferred_element_type=F32)
+            both = (within + cross * carried[pl.ds(index, 1), :]) * owner
+            kept[pl.ds(index, 1), :] = jnp.sum(both, 0, keepdims=True)
+
+    retained = kept[...] + own * valued.astype(F32)
+    centred = retained - per_head(retained) * (1.0 / HDIM)
+    variance = per_head(centred * centred) * (1.0 / HDIM)
+    normed = centred * lax.rsqrt(variance + EPS) * gain[...]
+    mixed[...] = (jax.nn.silu(gated.astype(F32)) * normed).astype(BF16)
 
 
 def normalize(values, gain, mine, landed, sems):
@@ -273,7 +314,6 @@
     ]
     for load in loads:
         load.start()
-    enter(("tp", "kv"))
     nkv, seqs, width = heads.shape
     tp, kv = lax.axis_index("tp"), lax.axis_index("kv")
     ntp, block, depth = hidden_all.shape
@@ -432,11 +472,25 @@
     each_tile(wait_sends)
 
 
-def mixer(mixed, tokens, out_w, mixer_gain, up_w, down_w, final_gain):
+def layer_kernel(*refs):
+    tokens, weights, tables, caches, mixes = refs[0], refs[1:5], refs[5:10], refs[10:13], refs[13:18]
+    out, refs = refs[18], refs[19:]
+    (summed, *own), refs = refs[:8], refs[8:]
+    (mixed, keys, values, state, wide, kept, cache_sems), refs = refs[:7], refs[7:]
+    loads = load_caches(caches, (keys, values, state), cache_sems)
+    project_kernel(loads, tokens, *weights, summed, *own)
+    for load in loads:
+        load.wait()
+    retain_kernel(summed, *tables, mixed, keys, values, state, wide, kept)
+    mixer_kernel(mixed, tokens, *mixes, out, *refs)
+
+
+def layer(tokens, weights, tables, caches, mixes):
     ntp, nkv = lax.axis_size("tp"), lax.axis_size("kv")
-    seqs, width = mixed.shape
     block, depth = tokens.shape
-    inner = up_w.shape[1]
+    width = weights[0].shape[1]
+    seqs = caches[0].shape[0]
+    inner = mixes[2].shape[1]
     chips = ntp // PAIR
     side = math.isqrt(nkv)
     tile = min(TILE, inner)
@@ -444,12 +498,25 @@
     vmem, anyw = pl.BlockSpec(memory_space=pltpu.VMEM), pl.BlockSpec(memory_space=pl.ANY)
     dma = pltpu.SemaphoreType.DMA
     return pl.pallas_call(
-        mixer_kernel,
-        name="mixer",
+        layer_kernel,
+        name="layer",
         out_shape=jax.ShapeDtypeStruct((block, depth), BF16),
-        in_specs=[vmem, vmem, anyw, vmem, anyw, anyw, vmem],
+        in_specs=[vmem] + [anyw] * 4 + [vmem] * 5 + [anyw] * 3 + [anyw, vmem, anyw, anyw, vmem],
         out_specs=vmem,
         scratch_shapes=[
+            pltpu.VMEM((seqs, 4 * width), BF16),
+            pltpu.VMEM((ntp, block, depth), BF16),
+            pltpu.VMEM((4, depth, width), BF16),
+            pltpu.VMEM((4, nkv, seqs, width), BF16),
+            pltpu.VMEM((4, nkv - 1, seqs, width), BF16),
+            dma((2, ntp - 1)),
+            dma((2, 4, nkv - 1)),
+            dma((4,)),
+            pltpu.VMEM((seqs, width), BF16),
+            *[pltpu.VMEM(cache.shape, cache.dtype) for cache in caches],
+            pltpu.VMEM((seqs, HEAD_ROWS, width), F32),
+            pltpu.VMEM((seqs, width), F32),
+            dma((3,)),
             pltpu.VMEM((width, depth), BF16),
             pltpu.VMEM((depth, inner), BF16),
             pltpu.VMEM((inner, depth), BF16),
@@ -478,50 +545,26 @@
             dma((2, ntp - 1)),
         ],
         compiler_params=pltpu.CompilerParams(
-            collective_id=1, has_side_effects=True, vmem_limit_bytes=60 * 2**20
+            collective_id=0, has_side_effects=True, vmem_limit_bytes=60 * 2**20
         ),
-    )(mixed, tokens, out_w, mixer_gain[None, :], up_w, down_w, final_gain[None, :])
-
-
-def rotate(vectors, positions):
-    half = vectors.shape[-1] // 2
+    )(tokens, *weights, *tables, *caches, *mixes)
+
+
+def tables_of(lengths, rate, gain):
+    heads = rate.shape[0]
+    half = HDIM // 2
     inverse = 10000.0 ** (-jnp.arange(half, dtype=F32) / half)
-    angle = positions.astype(F32)[:, None] * inverse[None, :]
-    cosine = jnp.cos(angle)[:, None, :]
-    sine = jnp.sin(angle)[:, None, :]
-    former, latter = (vectors[..., :half], vectors[..., half:])
-    return jnp.concatenate([former * cosine - latter * sine, latter * cosine + former * sine], -1)
-
-
-def retain(query, keyed, valued, gated, lengths, state, keys, values, rate, gain):
-    count, width = query.shape
-    heads = rate.shape[0]
-    q_rot = rotate(query.astype(F32).reshape(count, heads, HDIM), lengths).astype(BF16)
-    k_rot = (rotate(keyed.astype(F32).reshape(count, heads, HDIM), lengths) * 0.125).astype(BF16)
-    v_new = valued.astype(F32).reshape(count, heads, HDIM)
-    owner = jnp.arange(width, dtype=jnp.int32)[None, :] // HDIM == jnp.arange(heads)[:, None]
-    q_wide = jnp.where(owner[None], q_rot.reshape(count, 1, width), jnp.zeros((), BF16))
-    scores = jnp.einsum("shc,sic->shi", q_wide, keys, preferred_element_type=F32)
+    angle = lengths.astype(F32)[:, None] * inverse[None, :]
+    cos = jnp.tile(jnp.cos(angle), (1, 2 * heads))
+    sin = jnp.tile(jnp.sin(angle), (1, 2 * heads))
     offset = lengths % BLK
     slots = jnp.arange(BLK, dtype=jnp.int32)
     lag = jnp.maximum(offset[:, None] - slots[None, :], 0).astype(F32)
     live = (slots[None, :] < offset[:, None])[:, None, :]
-    factor = jnp.where(live, jnp.exp(-rate[None, :, None] * lag[:, None, :]), 0.0)
-    weights = (scores * factor).astype(BF16)
-    own = jnp.einsum("shn,shn->sh", q_rot, k_rot, preferred_element_type=F32).astype(BF16)
-    inner = jnp.einsum("shi,sic->shc", weights, values, preferred_element_type=F32)
-    carried = jnp.exp(-rate[None, :] * (offset[:, None] + 1).astype(F32))
-    cross = jnp.einsum(
-        "shk,skc->shc", q_rot, state.astype(BF16), preferred_element_type=F32
-    )
-    both = jnp.sum(jnp.where(owner[None], inner + cross * carried[..., None], 0.0), 1)
-    retained = both.reshape(count, heads, HDIM) + own.astype(F32)[..., None] * v_new
-    mean = jnp.mean(retained, -1, keepdims=True)
-    centred = retained - mean
-    spread = jnp.mean(centred * centred, -1, keepdims=True)
-    normed = centred * lax.rsqrt(spread + EPS) * gain.reshape(heads, HDIM)[None]
-    gate_f = jax.nn.silu(gated.astype(F32).reshape(count, heads, HDIM))
-    return (gate_f * normed).reshape(count, heads * HDIM).astype(BF16)
+    padded = jnp.pad(rate, (0, HEAD_ROWS - heads))
+    factor = jnp.where(live, jnp.exp(-padded[None, :, None] * lag[:, None, :]), 0.0)
+    carried = jnp.exp(-jnp.repeat(rate, HDIM)[None, :] * (offset[:, None] + 1).astype(F32))
+    return cos, sin, carried, factor, gain[None, :]
 
 
 def per_device(
@@ -542,24 +585,13 @@
     down_weight,
     final_gain,
 ):
-    width = query_weight.shape[1]
-    summed = project(tokens, query_weight, key_weight, value_weight, gate_weight)
-    query, keyed, valued, gated = [
-        summed[:, index * width : (index + 1) * width] for index in range(4)
-    ]
-    mixed = retain(
-        query,
-        keyed,
-        valued,
-        gated,
-        lengths,
-        state_block,
-        cached_keys,
-        cached_values,
-        decay_rate,
-        head_gain,
+    return layer(
+        tokens,
+        (query_weight, key_weight, value_weight, gate_weight),
+        tables_of(lengths, decay_rate, head_gain),
+        (cached_keys, cached_values, state_block),
+        (out_weight, mixer_gain[None, :], up_weight, down_weight, final_gain[None, :]),
     )
-    return mixer(mixed, tokens, out_weight, mixer_gain, up_weight, down_weight, final_gain)
 
 
 def solution(mesh):

time: 98.6 us -> 98.8 us (level)
  Pallas kernels: 83.5 us -> 91.5 us
  matrix products: 7.8 us -> 0 us
    pallas_call x2 -> x1, Pallas kernels: 83.5 us -> 91.5 us  [layer(): pl.pallas_call(layer_kernel, name='layer', out_shape=jax.ShapeDtypeStruct...]
    dot_general x2 -> x0, matrix products: 7.8 us -> none  [the longest x1 5.2 us: retain(): jnp.einsum('shi,sic->shc', weights, values, preferred_element_type=F32)]
    convert_element_type x5 -> x2, other arithmetic: 2.28 us -> 0.82 us  [the longest x1 0.74 us: tables_of(): (offset[:, None] + 1).astype(F32)]
    another operation x0 -> x4, local copies, waits for them, and re-layouts: none -> 1.44 us  [the longest x2 0.72 us: tables_of(): cos = jnp.tile(jnp.cos(angle), (1, 2 * heads))]
    neg x1 -> x2, other arithmetic: 0.01 us -> 1.32 us  [the longest x1 0.66 us: tables_of(): -padded[None, :, None] * lag[:, None, :]]
where the time goes in v4:
time: 98.8 us; the launch traced here: 98.6 us
  Pallas kernels  91.5 us (93%)
  other arithmetic  4 us (4%)
  local copies, waits for them, and re-layouts  3.06 us (3%)
    pallas_call x1, Pallas kernels, layer(): pl.pallas_call(layer_kernel, name='layer', out_shape=jax.ShapeDtypeStruct...  91.5 us

profile of v4, /device:TPU:0, one launch (start us, length us, event | category | flops | bytes accessed | tf_op | source)
XLA Modules:
  0.0 98.6 jit_solution(3807642299139707532)
XLA Ops:
  0.0 0.7 pad_negate_fusion
  0.7 0.7 neg.24
  1.3 0.1 broadcast_in_dim.20
  1.4 0.1 neg.25
  1.5 0.7 add_convert_fusion
  2.2 0.1 iota_compare_fusion
  2.3 0.1 maximum_convert_fusion
  2.4 0.1 multiply_sine_fusion
  2.5 0.7 multiply_exponential_fusion.refs_7_
  3.2 0.7 copy.18.refs_6_
  4.0 0.7 copy.17.refs_5_
  4.7 0.9 exponential_select_fusion.refs_8_
  5.6 91.5 %layer.1 = bf16[32,1024]{1,0:T(8,128)(2,1)} custom-call(bf16[32,1024]{1,0:T(8,128)(2,1)} %refs_0_.1, bf16[1024,256]{1,0:T(8,128)(2,1)} %refs_1_.1, bf16[1024,256]{1,0:T(8,128)(2,1)} %refs_2_.1, bf16[1024,256]{1,0:T(8,128)(2,1)} %refs_3_.1, bf16[1024,256]{1,0:T(8,128)(2,1)} %refs_4_.1, f32[64,256]{1,0:T(8,128)} %copy.17.refs_5_, f32[64,256]{1,0:T(8,128)} %copy.18.refs_6_, ...), custom_call_target="tpu_custom_call" | custom-call | tf_op jit(solution)/shard_map/layer/pallas_call | solution.py:500
  97.2 1.5 %copy.20 = bf16[32,1024]{1,0:T(8,128)(2,1)} copy(bf16[32,1024]{1,0:T(8,128)(2,1)} %layer.1) | data formatting | bytes 131072
  (3 shorter events, 0.0 us)
